TPU v7x, 256 devices: a whole 4x4x8 slice. The times are simulated.
256 devices in a mesh: sp: 64 (over z, x, core), tp: 4 (over y).
Axes of the slice: x: 4, y: 4, z: 8, core: 2. Of those that a mesh axis runs over, the one named last changes fastest.
Arguments:
- stream: bfloat16 [32768, 2048], P(('sp', 'tp')), may hold values from -6 to 6
- pool_in: bfloat16 [32768, 1024], P('sp', 'tp'), may hold values from -6 to 6
- doc_ids: int32 [32768], P('sp'), may hold values from 0 to 7, never falling along the last dimension, each value on 1 to 8192 neighbouring positions
- pool_map: bfloat16 [4, 256, 512], P('tp'), may hold values from -0.375 to 0.375
- pool_scale: float32 [2048], P('tp'), may hold values from 0.1 to 1.9
- out_weight: bfloat16 [2048, 2048], P('tp'), may hold values from -0.125 to 0.125
- norm_gain: float32 [2048], replicated, may hold values from 0.1 to 1.9
- routes: int32 [32768, 2], P('sp'), may hold values from 0 to 63, all different within a row; in each aligned block of 128 rows (0 to 127, 128 to 255, ...) at most 6 rows name the same one
- route_weight: float32 [32768, 2], P(('sp', 'tp')), may hold values from 0.2 to 1
- expert_gate: bfloat16 [64, 2048, 1024], P('sp', None, 'tp'), may hold values from -0.125 to 0.125
- expert_up: bfloat16 [64, 2048, 1024], P('sp', None, 'tp'), may hold values from -0.125 to 0.125
- expert_down: bfloat16 [64, 1024, 2048], P('sp', 'tp'), may hold values from -0.1875 to 0.1875
Outputs:
- result: bfloat16 [32768, 2048], P(('sp', 'tp'))
Inputs may be any that keep to these rules, and one draw needn't show every extreme that they name: `routes`: each token names 2 different experts; in each aligned block of 128 rows no expert is named by more than 6 rows, a bound that some block reaches. `doc_ids`: never falling; each document holds at most 8192 positions.
All inputs are finite; a program needn't handle non-finite values.
Results may differ from a plain program's by a relative error of at most 0.014.
Values may be sent and summed in bfloat16 or wider, within the bound.
A program may use at most 64 MiB of HBM per device.

v0:
```python
import jax
import jax.numpy as jnp
from jax import lax
from jax.sharding import PartitionSpec as P

SPAN = 16
EPS = 1e-06


def passed_along(value, axis, by):
    length = lax.axis_size(axis)
    pairs = [(i, i + by) for i in range(length) if 0 <= i + by < length]
    return lax.ppermute(value, axis, pairs)


def cut_along(value, dim, length):
    before, after = (value.shape[:dim], value.shape[dim + 1 :])
    return jnp.moveaxis(value.reshape(*before, length, -1, *after), dim, 0)


def sum_at_owner(value, axis, dim):
    length = lax.axis_size(axis)
    tiles = lax.all_to_all(cut_along(value, dim, length), axis, 0, 0, tiled=True)
    return jnp.sum(tiles.astype(jnp.float32), axis=0)


def slot_table(route_block, expert_count, capacity, top_count):
    flattened = route_block.reshape(-1)
    one_hot = (flattened[:, None] == jnp.arange(expert_count, dtype=jnp.int32)[None, :]).astype(
        jnp.int32
    )
    ranking = jnp.sum((jnp.cumsum(one_hot, axis=0) - one_hot) * one_hot, axis=1)
    target_slot = flattened * capacity + ranking
    matches = target_slot[None, :] == jnp.arange(expert_count * capacity, dtype=jnp.int32)[:, None]
    sources = jnp.sum(
        jnp.where(matches, jnp.arange(flattened.shape[0], dtype=jnp.int32)[None, :], 0), axis=1
    )
    filled = jnp.any(matches, axis=1)
    return (target_slot, sources // top_count, filled)


def per_device(
    stream,
    pool_in,
    doc_ids,
    pool_map,
    pool_scale,
    out_weight,
    norm_gain,
    routes,
    route_weight,
    expert_gate,
    expert_up,
    expert_down,
):
    row_count = pool_in.shape[0]
    model_width = stream.shape[1]
    top_count = routes.shape[1]
    tp_count = lax.axis_size("tp")
    expert_count = lax.axis_size("sp")
    quarter = row_count // tp_count
    capacity = max(2, 3 * top_count * quarter // (2 * expert_count))
    all_gate = lax.all_gather(expert_gate, "tp", axis=0, tiled=True)
    all_up = lax.all_gather(expert_up, "tp", axis=0, tiled=True)
    all_down = lax.all_gather(expert_down, "tp", axis=0, tiled=True)
    reach_rows = SPAN - 1
    tail_rows = (
        pool_in[row_count - reach_rows :],
        doc_ids[row_count - reach_rows :].astype(jnp.bfloat16),
    )
    prior_rows, prior_docs = passed_along((tail_rows[0], tail_rows[1]), "sp", 1)
    extended = jnp.concatenate([prior_rows, pool_in], axis=0).astype(jnp.float32)
    extended_docs = jnp.concatenate([prior_docs.astype(jnp.float32), doc_ids.astype(jnp.float32)])
    own_docs = doc_ids.astype(jnp.float32)
    window = jnp.left_shift(jnp.int32(2), lax.axis_index("tp"))
    positions = lax.axis_index("sp") * row_count + jnp.arange(row_count, dtype=jnp.int32)
    running = jnp.zeros(pool_in.shape, jnp.float32)
    counts = jnp.zeros((row_count,), jnp.float32)
    for offset in range(reach_rows + 1):
        begin_row = reach_rows - offset
        piece_rows = extended[begin_row : begin_row + row_count]
        piece_docs = extended_docs[begin_row : begin_row + row_count]
        in_window = (offset < window) & (positions - offset >= 0) & (piece_docs == own_docs)
        running = running + jnp.where(in_window[:, None], piece_rows, 0.0)
        counts = counts + in_window.astype(jnp.float32)
    pooled = (running / counts[:, None] - pool_in.astype(jnp.float32)).astype(jnp.bfloat16)
    branch = (jnp.dot(pooled, pool_map[0], preferred_element_type=jnp.float32) * pool_scale).astype(
        jnp.bfloat16
    )
    projected = sum_at_owner(
        jnp.dot(branch, out_weight, preferred_element_type=jnp.float32).astype(jnp.bfloat16),
        "tp",
        0,
    )
    mixed_rows = (stream.astype(jnp.float32) + projected).astype(jnp.bfloat16)
    mixed_up = mixed_rows.astype(jnp.float32)
    normed = (
        mixed_up * lax.rsqrt(jnp.mean(mixed_up * mixed_up, axis=1, keepdims=True) + EPS) * norm_gain
    ).astype(jnp.bfloat16)
    own_routes = lax.dynamic_slice_in_dim(routes, lax.axis_index("tp") * quarter, quarter, 0)
    own_slots, own_sources, own_filled = slot_table(own_routes, expert_count, capacity, top_count)
    token_index = own_sources.reshape(expert_count, 1, capacity)
    filled_slots = own_filled.reshape(expert_count, 1, capacity)
    dispatch = jnp.where(filled_slots[..., None], normed[token_index], jnp.zeros((), jnp.bfloat16))
    arrived = lax.all_to_all(dispatch, "sp", split_axis=0, concat_axis=0, tiled=True)
    stacked = arrived.reshape(-1, model_width)
    expert_sum = jnp.zeros(stacked.shape, jnp.float32)
    for part in range(tp_count):
        gate_pre = jnp.dot(stacked, all_gate[part], preferred_element_type=jnp.float32)
        up_pre = jnp.dot(stacked, all_up[part], preferred_element_type=jnp.float32)
        hidden = (jax.nn.silu(gate_pre) * up_pre).astype(jnp.bfloat16)
        part_out = jnp.dot(hidden, all_down[part], preferred_element_type=jnp.float32)
        expert_sum = expert_sum + part_out.astype(jnp.bfloat16).astype(jnp.float32)
    summed = expert_sum.astype(jnp.bfloat16).reshape(arrived.shape)
    returned = lax.all_to_all(summed, "sp", split_axis=0, concat_axis=0, tiled=True)
    outputs = returned.reshape(expert_count * capacity, model_width)
    picked = outputs[own_slots].astype(jnp.float32).reshape(quarter, top_count, model_width)
    combined = jnp.sum(route_weight[:, :, None] * picked, axis=1)
    return (mixed_up + combined).astype(jnp.bfloat16)


def solution(mesh):
    in_specs = (
        P(("sp", "tp"), None),
        P("sp", "tp"),
        P("sp"),
        P("tp", None, None),
        P("tp"),
        P("tp", None),
        P(),
        P("sp", None),
        P(("sp", "tp"), None),
        P("sp", None, "tp"),
        P("sp", None, "tp"),
        P("sp", "tp", None),
    )
    out_specs = P(("sp", "tp"), None)
    return jax.shard_map(
        per_device, mesh=mesh, in_specs=in_specs, out_specs=out_specs, check_vma=False
    )
```

profile of v0, /device:TPU:2, one launch (start us, length us, event | category | flops | bytes accessed | tf_op | source)
XLA Modules:
  0.0 302.6 jit_solution(7720405257235284247)
XLA Ops:
  6.5 0.0 copy-start
  6.5 0.0 all-gather.4.cloned.1.call-start
  6.6 0.7 all-gather.4.cloned.1.call-update
  7.3 0.0 all-gather.6.cloned.1.call-start
  7.3 0.7 all-gather.6.cloned.1.call-update
  8.1 0.1 slice.144
  8.1 1.9 collective-permute-start.1
  10.1 3.5 %collective-permute-start = (bf16[15,256]{1,0:T(8,128)(2,1)S(1)}, bf16[15,256]{1,0:T(8,128)(2,1)S(1)}, u32[]{:S(2)}, u32[]{:S(2)}) collective-permute-start(bf16[15,256]{1,0:T(8,128)(2,1)S(1)} %slice.142), channel_id=1, source_target_pairs={{0,4},{4,8},{8,12},{12,16},{16,20},{20,24},{24,28},{28,32},{32,36}... | collective-permute-start | bytes 23048 | tf_op jit(solution)/shard_map/ppermute | solution.py:13
  13.6 0.0 collective-permute-done.1
  13.6 0.1 pad_maximum_fusion
  13.7 0.1 convert_add_fusion.1
  13.8 1.2 collective-permute-done
  15.0 0.1 maximum_convert_fusion
  15.1 0.0 copy-done
  15.1 0.0 copy-done.8
  15.1 0.0 copy-done.7
  15.1 4.4 %convolution_convert_fusion = bf16[512,2048]{1,0:T(8,128)(2,1)} fusion(bf16[512,2048]{1,0:T(8,128)(2,1)S(1)} %copy-done, f32[512]{0:T(512)S(1)} %copy-done.8, bf16[512,256]{1,0:T(8,128)(2,1)S(1)} %copy-done.2, f32[527,256]{1,0:T(8,128)S(1)} %maximum_convert_fusion, bf16[1,256,512]{2,1,0:T(8,128)(2,1)S(1)} %copy-done.7, f32[512]{0:T(512)S(1)} %get-tuple-element.9, ...), kind=kOutput, calls=%fused_computation.4 | convolution fusion | flops 1214119936 | bytes 13119488 | tf_op jit(solution)/shard_map/dot_general | solution.py:91
  19.6 4.5 %all-to-all-start = ((bf16[4,128,2048]{2,1,0:T(8,128)(2,1)}), bf16[4,128,2048]{2,1,0:T(8,128)(2,1)}, u32[]{:S(2)}, u32[]{:S(2)}) async-start(bf16[4,128,2048]{2,1,0:T(8,128)(2,1)} %bitcast.84), calls=%async_computation | async-start | bytes 4194304 | tf_op jit(solution)/shard_map/all_to_all | solution.py:23
  24.0 0.0 all-gather.8.cloned.1.call-start
  24.1 0.7 all-gather.8.cloned.1.call-update
  24.8 0.7 broadcast_multiply_fusion
  25.5 0.1 copy.27
  25.6 0.1 reshape.206
  25.7 0.1 eq.103
  25.9 0.6 reduce-window.6
  26.5 0.2 slice_reduce_fusion
  26.7 0.1 fusion.99
  26.9 0.2 fusion.52
  27.0 0.2 broadcast_in_dim.172
  27.2 0.2 select_reduce_fusion
  27.3 0.1 reduce_sum.53
  27.5 0.1 reshape.214
  27.7 0.0 copy-start.3
  27.7 45.3 %all-to-all-done = bf16[4,128,2048]{2,1,0:T(8,128)(2,1)} async-done(((bf16[4,128,2048]{2,1,0:T(8,128)(2,1)}), bf16[4,128,2048]{2,1,0:T(8,128)(2,1)}, u32[]{:S(2)}, u32[]{:S(2)}) %all-to-all-start) | async-done | bytes 2097184 | tf_op jit(solution)/shard_map/all_to_all | solution.py:23
  73.0 2.1 convert_reduce_fusion
  75.1 1.3 fusion.5
  76.4 0.0 copy-done.3
  76.4 0.2 fusion.7
  76.6 3.1 %gather_fusion = bf16[384,2048]{1,0:T(8,128)(2,1)} fusion(bf16[128,2048]{1,0:T(8,128)(2,1)S(1)} %fusion.7, s32[1024]{0:T(1024)S(1)} %pad_clamp_fusion.1), kind=kCustom, calls=%fused_computation | custom fusion | bytes 3147264 | tf_op jit(solution)/shard_map/gather | solution.py:104
  79.8 3.7 %reshape.213 = bf16[64,1,6,2048]{3,2,0,1:T(8,128)(2,1)} reshape(bf16[384,2048]{1,0:T(8,128)(2,1)} %gather_fusion) | data formatting | bytes 3145728 | tf_op jit(solution)/shard_map/gather | solution.py:104
  83.4 1.8 select_bitcast_fusion
  85.3 63.9 %all_to_all.15 = bf16[64,1,6,2048]{3,2,1,0:T(8,128)(2,1)} all-to-all(bf16[64,1,6,2048]{3,2,1,0:T(8,128)(2,1)S(1)} %select_bitcast_fusion), channel_id=1, replica_groups=mesh['sp'=64,'tp'=4] {'sp'}, dimensions={0} | all-to-all | bytes 3145728 | tf_op jit(solution)/shard_map/all_to_all | solution.py:105
  149.2 3.7 %reshape.208 = bf16[384,2048]{1,0:T(8,128)(2,1)} reshape(bf16[64,1,6,2048]{3,2,1,0:T(8,128)(2,1)} %all_to_all.15) | data formatting | bytes 3145728 | tf_op jit(solution)/shard_map/reshape | solution.py:106
  152.9 3.3 %fusion.9 = f32[384,256]{1,0:T(8,128)} fusion(bf16[384,2048]{1,0:T(8,128)(2,1)} %reshape.208, bf16[4,2048,256]{2,1,0:T(8,128)(2,1)} %all-gather.4.cloned.1.call-done), kind=kOutput, calls=%fused_computation.31 | convolution fusion | flops 402653184 | bytes 3014656 | tf_op jit(solution)/shard_map/dot_general | solution.py:109
  156.2 2.7 fusion.10
  158.9 1.4 fusion.11
  160.3 0.6 fusion.12
  160.9 0.0 all-gather.6.cloned.1.call-done
  160.9 29.9 %all-gather.8.cloned.1.call-done = bf16[4,256,2048]{2,1,0:T(8,128)(2,1)} async-done(((bf16[1,256,2048]{2,1,0:T(8,128)(2,1)}), bf16[4,256,2048]{2,1,0:T(8,128)(2,1)}) %all-gather.8.cloned.1.call-update) | async-done | bytes 4194320 | tf_op jit(solution)/shard_map/all_gather | solution.py:65
  190.8 5.2 %convolution_convert_fusion.3 = bf16[384,2048]{1,0:T(8,128)(2,1)} fusion(bf16[384,2048]{1,0:T(8,128)(2,1)} %reshape.208, bf16[4,256,2048]{2,1,0:T(8,128)(2,1)} %all-gather.8.cloned.1.call-done, bf16[4,2048,256]{2,1,0:T(8,128)(2,1)} %all-gather.6.cloned.1.call-done, f32[384,256]{1,0:T(8,128)} %fusion.11), kind=kOutput, calls=%fused_computation.7 | convolution fusion | flops 806682624 | bytes 5636096 | tf_op jit(solution)/shard_map/dot_general | solution.py:112
  196.0 5.1 %convolution_convert_fusion.2 = bf16[384,2048]{1,0:T(8,128)(2,1)} fusion(bf16[384,2048]{1,0:T(8,128)(2,1)} %reshape.208, bf16[4,256,2048]{2,1,0:T(8,128)(2,1)} %all-gather.8.cloned.1.call-done, bf16[4,2048,256]{2,1,0:T(8,128)(2,1)} %all-gather.6.cloned.1.call-done, f32[384,256]{1,0:T(8,128)} %fusion.10), kind=kOutput, calls=%fused_computation.6 | convolution fusion | flops 806682624 | bytes 5636096 | tf_op jit(solution)/shard_map/dot_general | solution.py:112
  201.1 5.1 %convolution_convert_fusion.1 = bf16[384,2048]{1,0:T(8,128)(2,1)} fusion(bf16[384,2048]{1,0:T(8,128)(2,1)} %reshape.208, bf16[4,256,2048]{2,1,0:T(8,128)(2,1)} %all-gather.8.cloned.1.call-done, bf16[4,2048,256]{2,1,0:T(8,128)(2,1)} %all-gather.6.cloned.1.call-done, f32[384,256]{1,0:T(8,128)} %fusion.9), kind=kOutput, calls=%fused_computation.5 | convolution fusion | flops 806682624 | bytes 5636096 | tf_op jit(solution)/shard_map/dot_general | solution.py:112
  206.2 6.4 %add_convert_fusion = bf16[384,2048]{1,0:T(8,128)(2,1)} fusion(bf16[384,2048]{1,0:T(8,128)(2,1)} %convolution_convert_fusion.1, bf16[384,2048]{1,0:T(8,128)(2,1)} %convolution_convert_fusion.2, bf16[384,2048]{1,0:T(8,128)(2,1)} %convolution_convert_fusion.3, bf16[4,256,2048]{2,1,0:T(8,128)(2,1)} %all-gather.8.cloned.1.call-done, ...), kind=kOutput, calls=%fused_computation.3 | convolution fusion | flops 812974080 | bytes 10354688 | tf_op jit(solution)/shard_map/dot_general | solution.py:112
  212.6 3.7 %reshape.209 = bf16[64,1,6,2048]{3,2,0,1:T(8,128)(2,1)} reshape(bf16[384,2048]{1,0:T(8,128)(2,1)} %add_convert_fusion) | data formatting | bytes 3145728 | tf_op jit(solution)/shard_map/reshape | solution.py:114
  216.3 10.9 %all-to-all-start.2 = ((bf16[64,1,6,2048]{3,2,1,0:T(8,128)(2,1)}), bf16[64,1,6,2048]{3,2,1,0:T(8,128)(2,1)}, u32[]{:S(2)}, u32[]{:S(2)}) async-start(bf16[64,1,6,2048]{3,2,1,0:T(8,128)(2,1)} %bitcast.83), calls=%async_computation.2 | async-start | bytes 4194304 | tf_op jit(solution)/shard_map/all_to_all | solution.py:115
  227.2 0.1 copy.32
  227.3 0.1 mul.116
  227.4 0.1 copy.26
  227.6 50.7 %all-to-all-done.2 = bf16[64,1,6,2048]{3,2,1,0:T(8,128)(2,1)} async-done(((bf16[64,1,6,2048]{3,2,1,0:T(8,128)(2,1)}), bf16[64,1,6,2048]{3,2,1,0:T(8,128)(2,1)}, u32[]{:S(2)}, u32[]{:S(2)}) %all-to-all-start.2) | async-done | bytes 1572896 | tf_op jit(solution)/shard_map/all_to_all | solution.py:115
  278.3 3.7 %reshape.210 = bf16[384,2048]{1,0:T(8,128)(2,1)} reshape(bf16[64,1,6,2048]{3,2,1,0:T(8,128)(2,1)} %all-to-all-done.2) | data formatting | bytes 3145728 | tf_op jit(solution)/shard_map/reshape | solution.py:116
  282.0 4.9 %gather_fusion.1 = bf16[256,2048]{1,0:T(8,128)(2,1)} fusion(bf16[384,2048]{1,0:T(8,128)(2,1)} %reshape.210, s32[1024]{0:T(1024)S(1)} %pad_clamp_fusion), kind=kCustom, calls=%fused_computation.1 | custom fusion | bytes 2098176 | tf_op jit(solution)/shard_map/gather | solution.py:117
  286.9 3.4 %reshape.211 = f32[128,2,2048]{2,1,0:T(2,128)} reshape(bf16[256,2048]{1,0:T(8,128)(2,1)} %gather_fusion.1) | data formatting | bytes 3145728 | tf_op jit(solution)/shard_map/convert_element_type | solution.py:117
  290.3 4.8 %multiply_reduce_fusion = f32[128,2048]{1,0:T(8,128)S(1)} fusion(f32[128,2,2048]{2,1,0:T(2,128)} %reshape.211, f32[128,2]{1,0:T(8,128)S(1)} %copy.26), kind=kLoop, calls=%fused_computation.9 | loop fusion | flops 786432 | bytes 3146752 | tf_op jit(solution)/shard_map/reduce_sum | solution.py:118
  295.1 0.9 fusion.8
  (25 shorter events, 0.2 us)
Async XLA Ops:
  6.5 8.6 %copy-start = (bf16[512,2048]{1,0:T(8,128)(2,1)S(1)}, bf16[512,2048]{1,0:T(8,128)(2,1)}, u32[]{:S(2)}) copy-start(bf16[512,2048]{1,0:T(8,128)(2,1)} %param.17) | copy-start | bytes 6291460
  6.5 1.5 copy-start.4
  6.5 3.5 %copy-start.2 = (bf16[512,256]{1,0:T(8,128)(2,1)S(1)}, bf16[512,256]{1,0:T(8,128)(2,1)}, u32[]{:S(2)}) copy-start(bf16[512,256]{1,0:T(8,128)(2,1)} %param.13) | copy-start | bytes 786436
  6.5 8.6 %copy-start.8 = (f32[512]{0:T(512)S(1)}, f32[512]{0:T(512)}, u32[]{:S(2)}) copy-start(f32[512]{0:T(512)} %param.16) | copy-start | bytes 6148
  6.5 8.6 %copy-start.7 = (bf16[1,256,512]{2,1,0:T(8,128)(2,1)S(1)}, bf16[1,256,512]{2,1,0:T(8,128)(2,1)}, u32[]{:S(2)}) copy-start(bf16[1,256,512]{2,1,0:T(8,128)(2,1)} %param.15) | copy-start | bytes 786436
  6.5 146.4 %all-gather.4.cloned.1.call-start = ((), (), s32[]{:S(2)}) async-start(), calls=%async_computation.3 | async-start | bytes 5242880 | tf_op jit(solution)/shard_map/all_gather | solution.py:63
  7.3 153.6 %all-gather.6.cloned.1.call-start = ((), (), s32[]{:S(2)}) async-start(), calls=%async_computation.4 | async-start | bytes 5242880 | tf_op jit(solution)/shard_map/all_gather | solution.py:64
  8.1 5.5 %collective-permute-start.1 = (bf16[15]{0:T(256)(128)(2,1)S(1)}, bf16[15]{0:T(256)(128)(2,1)S(1)}, u32[]{:S(2)}, u32[]{:S(2)}) collective-permute-start(bf16[15]{0:T(256)(128)(2,1)S(1)} %slice.144), channel_id=1, source_target_pairs={{0,4},{4,8},{8,12},{12,16},{16,20},{20,24},{24,28},{28,32},{32,36}... | collective-permute-start | bytes 98 | tf_op jit(solution)/shard_map/ppermute | solution.py:13
  10.1 5.0 %collective-permute-start = (bf16[15,256]{1,0:T(8,128)(2,1)S(1)}, bf16[15,256]{1,0:T(8,128)(2,1)S(1)}, u32[]{:S(2)}, u32[]{:S(2)}) collective-permute-start(bf16[15,256]{1,0:T(8,128)(2,1)S(1)} %slice.142), channel_id=1, source_target_pairs={{0,4},{4,8},{8,12},{12,16},{16,20},{20,24},{24,28},{28,32},{32,36}... | collective-permute-start | bytes 23048 | tf_op jit(solution)/shard_map/ppermute | solution.py:13
  19.6 53.4 %all-to-all-start = ((bf16[4,128,2048]{2,1,0:T(8,128)(2,1)}), bf16[4,128,2048]{2,1,0:T(8,128)(2,1)}, u32[]{:S(2)}, u32[]{:S(2)}) async-start(bf16[4,128,2048]{2,1,0:T(8,128)(2,1)} %bitcast.84), calls=%async_computation | async-start | bytes 4194304 | tf_op jit(solution)/shard_map/all_to_all | solution.py:23
  24.0 166.8 %all-gather.8.cloned.1.call-start = ((), (), s32[]{:S(2)}) async-start(), calls=%async_computation.5 | async-start | bytes 5242880 | tf_op jit(solution)/shard_map/all_gather | solution.py:65
  27.7 48.8 %copy-start.3 = (f32[2048]{0:T(1024)S(1)}, f32[2048]{0:T(1024)}, u32[]{:S(2)}) copy-start(f32[2048]{0:T(1024)} %param.18) | copy-start | bytes 24580
  152.9 3.3 %copy-start.1 = (bf16[384,2048]{1,0:T(8,128)(2,1)S(1)}, bf16[384,2048]{1,0:T(8,128)(2,1)}, u32[]{:S(2)}) copy-start(bf16[384,2048]{1,0:T(8,128)(2,1)} %reshape.208) | copy-start | bytes 4718596
  156.2 2.7 copy-start.6
  216.3 11.1 %copy-start.5 = (f32[128,2]{0,1:T(2,128)S(1)}, f32[128,2]{0,1:T(2,128)}, u32[]{:S(2)}) copy-start(f32[128,2]{0,1:T(2,128)} %param.20) | copy-start | bytes 3076
  216.3 62.0 %all-to-all-start.2 = ((bf16[64,1,6,2048]{3,2,1,0:T(8,128)(2,1)}), bf16[64,1,6,2048]{3,2,1,0:T(8,128)(2,1)}, u32[]{:S(2)}, u32[]{:S(2)}) async-start(bf16[64,1,6,2048]{3,2,1,0:T(8,128)(2,1)} %bitcast.83), calls=%async_computation.2 | async-start | bytes 4194304 | tf_op jit(solution)/shard_map/all_to_all | solution.py:115
Sparse Core Ops, SparseCore 0:
  9.2 75.0 all-gather.3
  86.1 51.7 all-gather.5
  139.7 51.1 all-gather.7
where the time goes:
time: 304 us; the launch traced here: 303 us
  waiting for transfers between devices  129 us (42%)
  blocking collectives  63.9 us (21%)
  matrix products  34.2 us (11%)
  local copies, waits for them, and re-layouts  27.7 us (9%)
  starting transfers between devices  20.9 us (7%)
  between operations  13.4 us (4%)
  other arithmetic  13.3 us (4%)
    all_to_all x1, blocking collectives, per_device(): lax.all_to_all(dispatch, 'sp', split_axis=0, concat_axis=0, tiled=True)  63.9 us
    all_to_all x1, waiting for transfers between devices, per_device(): lax.all_to_all(summed, 'sp', split_axis=0, concat_axis=0, tiled=True)  50.7 us
    all_to_all x1, waiting for transfers between devices, sum_at_owner(): lax.all_to_all(cut_along(value, dim, length), axis, 0, 0, tiled=True)  45.3 us
    all_gather x1, waiting for transfers between devices, per_device(): all_down = lax.all_gather(expert_down, 'tp', axis=0, tiled=True)  29.9 us
    dot_general x4, matrix products, per_device(): jnp.dot(hidden, all_down[part], preferred_element_type=jnp.float32)  21.8 us
    all_to_all x1, starting transfers between devices, per_device(): lax.all_to_all(summed, 'sp', split_axis=0, concat_axis=0, tiled=True)  10.9 us
    dot_general x4, matrix products, per_device(): jnp.dot(stacked, all_gate[part], preferred_element_type=jnp.float32)  7.93 us
    gather x2, local copies, waits for them, and re-layouts, per_device(): normed[token_index]  6.78 us
  transfers between devices with their start and end apart: 7, of which 4 were waited for; matrix products, arithmetic and copies ran while one was open for 11% of the time, Pallas kernels for 0%

commit v1 on v0

--- a/solution.py
+++ b/solution.py
@@ -62,7 +62,8 @@
     capacity = max(2, 3 * top_count * quarter // (2 * expert_count))
     all_gate = lax.all_gather(expert_gate, "tp", axis=0, tiled=True)
     all_up = lax.all_gather(expert_up, "tp", axis=0, tiled=True)
-    all_down = lax.all_gather(expert_down, "tp", axis=0, tiled=True)
+    copies = jnp.concatenate([expert_down] * lax.axis_size("tp"), axis=0)
+    all_down = lax.all_to_all(copies, "tp", 0, 0, tiled=True)
     reach_rows = SPAN - 1
     tail_rows = (
         pool_in[row_count - reach_rows :],

time: 304 us -> 317 us (1.043)
  waiting for transfers between devices: 129 us -> 135 us
  local copies, waits for them, and re-layouts: 27.7 us -> 30.9 us
    all_to_all x0 -> x1, waiting for transfers between devices: none -> 36 us  [per_device(): all_down = lax.all_to_all(copies, 'tp', 0, 0, tiled=True)]
    all_gather x1 -> x0, waiting for transfers between devices: 29.9 us -> none  [per_device(): all_down = lax.all_gather(expert_down, 'tp', axis=0, tiled=True)]
    all_to_all x0 -> x1, starting transfers between devices: none -> 5.12 us  [per_device(): all_down = lax.all_to_all(copies, 'tp', 0, 0, tiled=True)]
    all_to_all x1, starting transfers between devices: 10.9 us -> 7.16 us  [per_device(): lax.all_to_all(summed, 'sp', split_axis=0, concat_axis=0, tiled=True)]
  transfers between devices with their start and end apart: 7 -> 7, of which waited for: 4 -> 4; matrix products, arithmetic and copies ran while one was open for 11% -> 12% of each run, Pallas kernels for 0% -> 0%
where the time goes in v1:
time: 317 us; the launch traced here: 315 us
  waiting for transfers between devices  135 us (43%)
  blocking collectives  63.2 us (20%)
  matrix products  34.8 us (11%)
  local copies, waits for them, and re-layouts  30.9 us (10%)
  starting transfers between devices  22.3 us (7%)
  other arithmetic  15.6 us (5%)
  between operations  13.7 us (4%)
    all_to_all x1, blocking collectives, per_device(): lax.all_to_all(dispatch, 'sp', split_axis=0, concat_axis=0, tiled=True)  63.2 us
    all_to_all x1, waiting for transfers between devices, per_device(): lax.all_to_all(summed, 'sp', split_axis=0, concat_axis=0, tiled=True)  50.7 us
    all_to_all x1, waiting for transfers between devices, sum_at_owner(): lax.all_to_all(cut_along(value, dim, length), axis, 0, 0, tiled=True)  46.2 us
    all_to_all x1, waiting for transfers between devices, per_device(): all_down = lax.all_to_all(copies, 'tp', 0, 0, tiled=True)  36 us
    dot_general x4, matrix products, per_device(): jnp.dot(hidden, all_down[part], preferred_element_type=jnp.float32)  21.8 us
    dot_general x4, matrix products, per_device(): jnp.dot(stacked, all_gate[part], preferred_element_type=jnp.float32)  7.72 us
    all_to_all x1, starting transfers between devices, per_device(): lax.all_to_all(summed, 'sp', split_axis=0, concat_axis=0, tiled=True)  7.16 us
    gather x2, local copies, waits for them, and re-layouts, per_device(): normed[token_index]  6.83 us
  transfers between devices with their start and end apart: 7, of which 4 were waited for; matrix products, arithmetic and copies ran while one was open for 12% of the time, Pallas kernels for 0%

profile of v1, /device:TPU:2, one launch (start us, length us, event | category | flops | bytes accessed | tf_op | source)
XLA Modules:
  0.0 315.4 jit_solution(10292409412370250174)
XLA Ops:
  6.5 0.0 copy-start
  6.5 0.0 all-gather.3.cloned.1.call-start
  6.5 0.7 all-gather.3.cloned.1.call-update
  7.3 0.8 fusion.158
  8.0 0.1 slice.144
  8.1 1.9 collective-permute-start.1
  10.0 0.7 slice.142
  10.7 3.5 %collective-permute-start = (bf16[15,256]{1,0:T(8,128)(2,1)S(1)}, bf16[15,256]{1,0:T(8,128)(2,1)S(1)}, u32[]{:S(2)}, u32[]{:S(2)}) collective-permute-start(bf16[15,256]{1,0:T(8,128)(2,1)S(1)} %slice.142), channel_id=1, source_target_pairs={{0,4},{4,8},{8,12},{12,16},{16,20},{20,24},{24,28},{28,32},{32,36}... | collective-permute-start | bytes 23048 | tf_op jit(solution)/shard_map/ppermute | solution.py:13
  14.3 0.0 collective-permute-done.1
  14.3 0.1 pad_maximum_fusion
  14.4 0.8 convert_add_fusion.1
  15.1 0.5 collective-permute-done
  15.7 1.0 maximum_convert_fusion
  16.7 5.3 %convolution_convert_fusion = bf16[512,2048]{1,0:T(8,128)(2,1)} fusion(bf16[512,2048]{1,0:T(8,128)(2,1)S(1)} %copy-done, f32[512]{0:T(512)} %param.16, bf16[512,256]{1,0:T(8,128)(2,1)} %param.13, f32[527,256]{1,0:T(8,128)S(1)} %maximum_convert_fusion, bf16[1,256,512]{2,1,0:T(8,128)(2,1)} %param.15, f32[512]{0:T(512)S(1)} %get-tuple-element.9, ...), kind=kOutput, calls=%fused_computation.4 | convolution fusion | flops 1214119936 | bytes 13119488 | tf_op jit(solution)/shard_map/dot_general | solution.py:92
  22.0 4.5 %all-to-all-start = ((bf16[4,128,2048]{2,1,0:T(8,128)(2,1)}), bf16[4,128,2048]{2,1,0:T(8,128)(2,1)}, u32[]{:S(2)}, u32[]{:S(2)}) async-start(bf16[4,128,2048]{2,1,0:T(8,128)(2,1)} %bitcast.85), calls=%async_computation | async-start | bytes 4194304 | tf_op jit(solution)/shard_map/all_to_all | solution.py:23
  26.6 0.0 all-gather.5.cloned.1.call-start
  26.6 0.7 all-gather.5.cloned.1.call-update
  27.3 0.7 broadcast_multiply_fusion
  28.0 0.1 copy.27
  28.1 0.1 reshape.207
  28.3 0.1 eq.103
  28.4 0.6 reduce-window.6
  29.1 0.2 slice_reduce_fusion
  29.3 0.1 fusion.99
  29.4 0.2 fusion.52
  29.6 0.2 broadcast_in_dim.172
  29.7 0.2 select_reduce_fusion
  29.9 0.1 reduce_sum.53
  30.1 0.1 reshape.215
  30.2 0.0 copy-start.3
  30.2 46.2 %all-to-all-done = bf16[4,128,2048]{2,1,0:T(8,128)(2,1)} async-done(((bf16[4,128,2048]{2,1,0:T(8,128)(2,1)}), bf16[4,128,2048]{2,1,0:T(8,128)(2,1)}, u32[]{:S(2)}, u32[]{:S(2)}) %all-to-all-start) | async-done | bytes 2097184 | tf_op jit(solution)/shard_map/all_to_all | solution.py:23
  76.4 2.1 convert_reduce_fusion
  78.5 1.3 fusion.5
  79.8 0.2 fusion.7
  80.0 3.1 gather_fusion
  83.2 3.7 %reshape.214 = bf16[64,1,6,2048]{3,2,0,1:T(8,128)(2,1)} reshape(bf16[384,2048]{1,0:T(8,128)(2,1)} %gather_fusion) | data formatting | bytes 3145728 | tf_op jit(solution)/shard_map/gather | solution.py:105
  86.9 1.8 select_bitcast_fusion
  88.7 0.0 copy-start.2
  88.7 63.2 %all_to_all.20 = bf16[64,1,6,2048]{3,2,1,0:T(8,128)(2,1)} all-to-all(bf16[64,1,6,2048]{3,2,1,0:T(8,128)(2,1)S(1)} %select_bitcast_fusion), channel_id=1, replica_groups=mesh['sp'=64,'tp'=4] {'sp'}, dimensions={0} | all-to-all | bytes 3145728 | tf_op jit(solution)/shard_map/all_to_all | solution.py:106
  152.0 0.0 copy-done.2
  152.0 2.5 concatenate.11
  154.5 5.1 %all-to-all-start.2 = ((bf16[4,256,2048]{2,1,0:T(8,128)(2,1)}), bf16[4,256,2048]{2,1,0:T(8,128)(2,1)}, u32[]{:S(2)}, u32[]{:S(2)}) async-start(bf16[4,256,2048]{2,1,0:T(8,128)(2,1)} %concatenate.11), calls=%async_computation.2 | async-start | bytes 8388608 | tf_op jit(solution)/shard_map/all_to_all | solution.py:66
  159.6 3.7 %reshape.209 = bf16[384,2048]{1,0:T(8,128)(2,1)} reshape(bf16[64,1,6,2048]{3,2,1,0:T(8,128)(2,1)} %all_to_all.20) | data formatting | bytes 3145728 | tf_op jit(solution)/shard_map/reshape | solution.py:107
  163.3 3.1 fusion.9
  166.4 2.7 fusion.10
  169.1 0.0 copy-done.5
  169.1 1.3 fusion.11
  170.4 0.6 fusion.12
  171.0 36.0 %all-to-all-done.2 = bf16[4,256,2048]{2,1,0:T(8,128)(2,1)} async-done(((bf16[4,256,2048]{2,1,0:T(8,128)(2,1)}), bf16[4,256,2048]{2,1,0:T(8,128)(2,1)}, u32[]{:S(2)}, u32[]{:S(2)}) %all-to-all-start.2) | async-done | bytes 4194336 | tf_op jit(solution)/shard_map/all_to_all | solution.py:66
  207.0 5.1 %convolution_convert_fusion.1 = bf16[384,2048]{1,0:T(8,128)(2,1)} fusion(bf16[384,2048]{1,0:T(8,128)(2,1)} %reshape.209, bf16[4,256,2048]{2,1,0:T(8,128)(2,1)} %all-to-all-done.2, bf16[4,2048,256]{2,1,0:T(8,128)(2,1)} %all-gather.5.cloned.1.call-done, f32[384,256]{1,0:T(8,128)} %fusion.9), kind=kOutput, calls=%fused_computation.5 | convolution fusion | flops 806682624 | bytes 5636096 | tf_op jit(solution)/shard_map/dot_general | solution.py:113
  212.2 5.1 %convolution_convert_fusion.2 = bf16[384,2048]{1,0:T(8,128)(2,1)} fusion(bf16[384,2048]{1,0:T(8,128)(2,1)} %reshape.209, bf16[4,256,2048]{2,1,0:T(8,128)(2,1)} %all-to-all-done.2, bf16[4,2048,256]{2,1,0:T(8,128)(2,1)} %all-gather.5.cloned.1.call-done, f32[384,256]{1,0:T(8,128)} %fusion.10), kind=kOutput, calls=%fused_computation.6 | convolution fusion | flops 806682624 | bytes 5636096 | tf_op jit(solution)/shard_map/dot_general | solution.py:113
  217.3 5.1 %convolution_convert_fusion.3 = bf16[384,2048]{1,0:T(8,128)(2,1)} fusion(bf16[384,2048]{1,0:T(8,128)(2,1)} %reshape.209, bf16[4,256,2048]{2,1,0:T(8,128)(2,1)} %all-to-all-done.2, bf16[4,2048,256]{2,1,0:T(8,128)(2,1)} %all-gather.5.cloned.1.call-done, f32[384,256]{1,0:T(8,128)} %fusion.11), kind=kOutput, calls=%fused_computation.7 | convolution fusion | flops 806682624 | bytes 5636096 | tf_op jit(solution)/shard_map/dot_general | solution.py:113
  222.4 6.4 %add_convert_fusion = bf16[384,2048]{1,0:T(8,128)(2,1)} fusion(bf16[384,2048]{1,0:T(8,128)(2,1)} %convolution_convert_fusion.1, bf16[384,2048]{1,0:T(8,128)(2,1)} %convolution_convert_fusion.2, bf16[384,2048]{1,0:T(8,128)(2,1)} %convolution_convert_fusion.3, bf16[4,256,2048]{2,1,0:T(8,128)(2,1)} %all-to-all-done.2, bf16[384,2048]{1,0:T(8,128)(2,1)} %reshape.209, ...), kind=kOutput, calls=%fused_computation.3 | convolution fusion | flops 812974080 | bytes 10354688 | tf_op jit(solution)/shard_map/dot_general | solution.py:113
  228.8 3.7 %reshape.210 = bf16[64,1,6,2048]{3,2,0,1:T(8,128)(2,1)} reshape(bf16[384,2048]{1,0:T(8,128)(2,1)} %add_convert_fusion) | data formatting | bytes 3145728 | tf_op jit(solution)/shard_map/reshape | solution.py:115
  232.5 7.2 %all-to-all-start.3 = ((bf16[64,1,6,2048]{3,2,1,0:T(8,128)(2,1)}), bf16[64,1,6,2048]{3,2,1,0:T(8,128)(2,1)}, u32[]{:S(2)}, u32[]{:S(2)}) async-start(bf16[64,1,6,2048]{3,2,1,0:T(8,128)(2,1)} %bitcast.84), calls=%async_computation.3 | async-start | bytes 4194304 | tf_op jit(solution)/shard_map/all_to_all | solution.py:116
  239.7 0.1 copy.32
  239.8 0.1 mul.116
  239.9 0.1 copy.26
  240.1 50.7 %all-to-all-done.3 = bf16[64,1,6,2048]{3,2,1,0:T(8,128)(2,1)} async-done(((bf16[64,1,6,2048]{3,2,1,0:T(8,128)(2,1)}), bf16[64,1,6,2048]{3,2,1,0:T(8,128)(2,1)}, u32[]{:S(2)}, u32[]{:S(2)}) %all-to-all-start.3) | async-done | bytes 1572896 | tf_op jit(solution)/shard_map/all_to_all | solution.py:116
  290.8 3.7 %reshape.211 = bf16[384,2048]{1,0:T(8,128)(2,1)} reshape(bf16[64,1,6,2048]{3,2,1,0:T(8,128)(2,1)} %all-to-all-done.3) | data formatting | bytes 3145728 | tf_op jit(solution)/shard_map/reshape | solution.py:117
  294.5 4.9 %gather_fusion.1 = bf16[256,2048]{1,0:T(8,128)(2,1)} fusion(bf16[384,2048]{1,0:T(8,128)(2,1)} %reshape.211, s32[1024]{0:T(1024)S(1)} %pad_clamp_fusion), kind=kCustom, calls=%fused_computation.1 | custom fusion | bytes 2098176 | tf_op jit(solution)/shard_map/gather | solution.py:118
  299.4 3.4 %reshape.212 = f32[128,2,2048]{2,1,0:T(2,128)} reshape(bf16[256,2048]{1,0:T(8,128)(2,1)} %gather_fusion.1) | data formatting | bytes 3145728 | tf_op jit(solution)/shard_map/convert_element_type | solution.py:118
  302.8 4.8 %multiply_reduce_fusion = f32[128,2048]{1,0:T(8,128)S(1)} fusion(f32[128,2,2048]{2,1,0:T(2,128)} %reshape.212, f32[128,2]{1,0:T(8,128)S(1)} %copy.26), kind=kLoop, calls=%fused_computation.9 | loop fusion | flops 786432 | bytes 3146752 | tf_op jit(solution)/shard_map/reduce_sum | solution.py:119
  307.6 0.9 fusion.8
  (19 shorter events, 0.1 us)
Async XLA Ops:
  6.5 10.2 %copy-start = (bf16[512,2048]{1,0:T(8,128)(2,1)S(1)}, bf16[512,2048]{1,0:T(8,128)(2,1)}, u32[]{:S(2)}) copy-start(bf16[512,2048]{1,0:T(8,128)(2,1)} %param.17) | copy-start | bytes 6291460
  6.5 156.8 %all-gather.3.cloned.1.call-start = ((), (), s32[]{:S(2)}) async-start(), calls=%async_computation.4 | async-start | bytes 5242880 | tf_op jit(solution)/shard_map/all_gather | solution.py:63
  8.1 6.2 %collective-permute-start.1 = (bf16[15]{0:T(256)(128)(2,1)S(1)}, bf16[15]{0:T(256)(128)(2,1)S(1)}, u32[]{:S(2)}, u32[]{:S(2)}) collective-permute-start(bf16[15]{0:T(256)(128)(2,1)S(1)} %slice.144), channel_id=1, source_target_pairs={{0,4},{4,8},{8,12},{12,16},{16,20},{20,24},{24,28},{28,32},{32,36}... | collective-permute-start | bytes 98 | tf_op jit(solution)/shard_map/ppermute | solution.py:13
  10.7 5.0 %collective-permute-start = (bf16[15,256]{1,0:T(8,128)(2,1)S(1)}, bf16[15,256]{1,0:T(8,128)(2,1)S(1)}, u32[]{:S(2)}, u32[]{:S(2)}) collective-permute-start(bf16[15,256]{1,0:T(8,128)(2,1)S(1)} %slice.142), channel_id=1, source_target_pairs={{0,4},{4,8},{8,12},{12,16},{16,20},{20,24},{24,28},{28,32},{32,36}... | collective-permute-start | bytes 23048 | tf_op jit(solution)/shard_map/ppermute | solution.py:13
  22.0 54.4 %all-to-all-start = ((bf16[4,128,2048]{2,1,0:T(8,128)(2,1)}), bf16[4,128,2048]{2,1,0:T(8,128)(2,1)}, u32[]{:S(2)}, u32[]{:S(2)}) async-start(bf16[4,128,2048]{2,1,0:T(8,128)(2,1)} %bitcast.85), calls=%async_computation | async-start | bytes 4194304 | tf_op jit(solution)/shard_map/all_to_all | solution.py:23
  26.6 180.4 %all-gather.5.cloned.1.call-start = ((), (), s32[]{:S(2)}) async-start(), calls=%async_computation.5 | async-start | bytes 5242880 | tf_op jit(solution)/shard_map/all_gather | solution.py:64
  30.2 49.6 %copy-start.3 = (f32[2048]{0:T(1024)S(1)}, f32[2048]{0:T(1024)}, u32[]{:S(2)}) copy-start(f32[2048]{0:T(1024)} %param.18) | copy-start | bytes 24580
  88.7 63.2 %copy-start.2 = (bf16[1,256,2048]{2,1,0:T(8,128)(2,1)S(1)}, bf16[1,256,2048]{2,1,0:T(8,128)(2,1)}, u32[]{:S(2)}) copy-start(bf16[1,256,2048]{2,1,0:T(8,128)(2,1)} %param.23) | copy-start | bytes 3145732
  154.5 52.6 %all-to-all-start.2 = ((bf16[4,256,2048]{2,1,0:T(8,128)(2,1)}), bf16[4,256,2048]{2,1,0:T(8,128)(2,1)}, u32[]{:S(2)}, u32[]{:S(2)}) async-start(bf16[4,256,2048]{2,1,0:T(8,128)(2,1)} %concatenate.11), calls=%async_computation.2 | async-start | bytes 8388608 | tf_op jit(solution)/shard_map/all_to_all | solution.py:66
  163.3 3.1 copy-start.1
  166.4 2.7 copy-start.5
  232.5 7.4 %copy-start.4 = (f32[128,2]{0,1:T(2,128)S(1)}, f32[128,2]{0,1:T(2,128)}, u32[]{:S(2)}) copy-start(f32[128,2]{0,1:T(2,128)} %param.20) | copy-start | bytes 3076
  232.5 58.3 %all-to-all-start.3 = ((bf16[64,1,6,2048]{3,2,1,0:T(8,128)(2,1)}), bf16[64,1,6,2048]{3,2,1,0:T(8,128)(2,1)}, u32[]{:S(2)}, u32[]{:S(2)}) async-start(bf16[64,1,6,2048]{3,2,1,0:T(8,128)(2,1)} %bitcast.84), calls=%async_computation.3 | async-start | bytes 4194304 | tf_op jit(solution)/shard_map/all_to_all | solution.py:116
Sparse Core Ops, SparseCore 0:
  9.1 76.1 all-gather.2
  87.2 51.1 all-gather.4
